TPU v7x, 32 devices: a whole 2x2x4 slice. The times are simulated.
32 devices in a mesh: grp: 2 (over x), fs: 4 (over z), tp: 4 (over y, core).
Axes of the slice: x: 2, y: 2, z: 4, core: 2. Of those that a mesh axis runs over, the one named last changes fastest.
Arguments:
- stream: bfloat16 [2048, 2048], P(('grp', 'fs'), 'tp'), parts along dimension 0, may hold values from -80 to 80
- mixed: bfloat16 [2048, 2048], P(('grp', 'fs'), 'tp'), parts along dimension 0, may hold values from -6 to 6
- out_weight: bfloat16 [2048, 2048], P('fs', 'tp'), may hold values from -0.125 to 0.125
- norm_gain: bfloat16 [2048], P('tp'), may hold values from 0.099609375 to 1.8984375
- up_weight: bfloat16 [2048, 8192], P('fs', 'tp'), may hold values from -0.125 to 0.125
- down_weight: bfloat16 [8192, 2048], P('tp', 'fs'), may hold values from -0.09375 to 0.09375
Outputs:
- result: bfloat16 [2048, 2048], P(('grp', 'fs'), 'tp'), parts along dimension 0
There are 2 independent parts, one for each index of `grp`. A program takes and returns all parts, laid end to end along the dimension named above; an argument that names none is the same for every part. Nothing has to cross between parts.
All inputs are finite; a program needn't handle non-finite values.
Results may differ from a plain program's by a relative error of at most 0.01.
Values may be sent and summed in bfloat16 or wider, within the bound.
A program may use at most 64 MiB of HBM per device.

v0:
```python
import jax
import jax.numpy as jnp
from jax import lax
from jax.sharding import PartitionSpec as P

epsilon = 1e-06


def fold_product(left, portion):
    return jnp.dot(left, portion, preferred_element_type=jnp.float32)


def gathered_body(stream, mixed, out_weight, norm_gain, up_weight, down_weight):
    mixed_whole = lax.all_gather(mixed, "tp", axis=1, tiled=True)
    projected = fold_product(mixed_whole, lax.all_gather(out_weight, "fs", axis=0, tiled=True))
    resid = (stream.astype(jnp.float32) + projected).astype(jnp.bfloat16)
    widened = resid.astype(jnp.float32)
    resid_whole, gain_whole = (
        lax.all_gather(resid, "tp", axis=1, tiled=True),
        lax.all_gather(norm_gain, "tp", axis=0, tiled=True),
    )
    stream_wide = resid_whole.astype(jnp.float32)
    energy = jnp.mean(stream_wide * stream_wide, axis=1, keepdims=True)
    normed_whole = (
        stream_wide * lax.rsqrt(energy + epsilon) * gain_whole.astype(jnp.float32)
    ).astype(jnp.bfloat16)
    up_full = lax.all_gather(up_weight, "fs", axis=0, tiled=True)
    up_values = jnp.dot(normed_whole, up_full, preferred_element_type=jnp.float32)
    activated = jnp.square(jax.nn.relu(up_values)).astype(jnp.bfloat16)
    partials = jnp.dot(
        activated,
        lax.all_gather(down_weight, "fs", axis=1, tiled=True),
        preferred_element_type=jnp.float32,
    )
    branch = lax.psum_scatter(partials, "tp", scatter_dimension=1, tiled=True)
    return (widened + branch).astype(jnp.bfloat16)


def spread_body(stream, mixed, out_weight, norm_gain, up_weight, down_weight):
    mixed_whole = lax.all_gather(mixed, "tp", axis=1, tiled=True)
    out_full = lax.all_gather(out_weight, "fs", axis=0, tiled=True)
    up_mine = lax.all_to_all(up_weight, "fs", split_axis=1, concat_axis=0, tiled=True)
    down_mine = lax.all_to_all(down_weight, "fs", split_axis=0, concat_axis=1, tiled=True)
    projected = jnp.dot(mixed_whole, out_full, preferred_element_type=jnp.float32)
    resid = (stream.astype(jnp.float32) + projected).astype(jnp.bfloat16)
    rows = lax.all_gather(resid, "fs", axis=0, tiled=True)
    whole = lax.all_gather(rows, "tp", axis=1, tiled=True).astype(jnp.float32)
    gain = lax.all_gather(norm_gain, "tp", axis=0, tiled=True).astype(jnp.float32)
    energy = jnp.mean(whole * whole, axis=1, keepdims=True)
    normed = (whole * lax.rsqrt(energy + epsilon) * gain).astype(jnp.bfloat16)
    up_values = jnp.dot(normed, up_mine, preferred_element_type=jnp.float32)
    activated = jnp.square(jax.nn.relu(up_values)).astype(jnp.bfloat16)
    partials = jnp.dot(activated, down_mine, preferred_element_type=jnp.float32).astype(
        jnp.bfloat16
    )
    columns = lax.psum_scatter(partials, "tp", scatter_dimension=1, tiled=True)
    branch = lax.psum_scatter(columns, "fs", scatter_dimension=0, tiled=True)
    return (resid.astype(jnp.float32) + branch.astype(jnp.float32)).astype(jnp.bfloat16)


def solution(mesh):
    placed = (
        P(("grp", "fs"), "tp"),
        P(("grp", "fs"), "tp"),
        P("fs", "tp"),
        P("tp"),
        P("fs", "tp"),
        P("tp", "fs"),
    )
    fs, tp = (mesh.shape["fs"], mesh.shape["tp"])

    def call(stream, mixed, out_weight, norm_gain, up_weight, down_weight):
        width, hidden = up_weight.shape
        tokens = stream.shape[0] // mesh.shape["grp"]
        moved_weights = 2 * width * hidden // tp
        moved_rows = 2 * tokens * width + 2 * width * hidden // (tp * fs)
        body = spread_body if moved_rows < moved_weights else gathered_body
        return sharded(body)(stream, mixed, out_weight, norm_gain, up_weight, down_weight)

    def sharded(body):
        return jax.shard_map(
            body, mesh=mesh, in_specs=placed, out_specs=P(("grp", "fs"), "tp"), check_vma=False
        )

    return call
```

profile of v0, /device:TPU:0, one launch (start us, length us, event | category | flops | bytes accessed | tf_op | source)
XLA Modules:
  0.0 298.6 jit_solution(17435808376531385950)
XLA Ops:
  6.5 0.0 all-gather.6.cloned.1.call-start
  6.5 0.7 all-gather.6.cloned.1.call-update
  7.3 0.0 all-gather.8.cloned.1.call-start
  7.3 0.7 all-gather.8.cloned.1.call-update
  8.0 0.0 all-gather.10.cloned.1.call-start
  8.1 20.3 %all-gather.6.cloned.1.call-done = bf16[256,2048]{1,0:T(8,128)(2,1)} async-done(((bf16[256,512]{1,0:T(8,128)(2,1)}), bf16[256,2048]{1,0:T(8,128)(2,1)}) %all-gather.6.cloned.1.call-update) | async-done | bytes 1048592 | tf_op jit(solution)/shard_map/all_gather | solution.py:40
  28.4 47.3 %all-gather.8.cloned.1.call-done = bf16[2048,512]{1,0:T(8,128)(2,1)} async-done(((bf16[512,512]{1,0:T(8,128)(2,1)}), bf16[2048,512]{1,0:T(8,128)(2,1)}) %all-gather.8.cloned.1.call-update) | async-done | bytes 2097168 | tf_op jit(solution)/shard_map/all_gather | solution.py:41
  75.6 3.3 %fusion.9 = bf16[256,512]{1,0:T(8,128)(2,1)} fusion(bf16[256,2048]{1,0:T(8,128)(2,1)} %all-gather.6.cloned.1.call-done, bf16[2048,512]{1,0:T(8,128)(2,1)} %all-gather.8.cloned.1.call-done, bf16[256,512]{1,0:T(8,128)(2,1)} %param.6), kind=kOutput, calls=%fused_computation.11 | convolution fusion | flops 537264128 | bytes 3670016 | tf_op jit(solution)/shard_map/dot_general | solution.py:44
  78.9 0.0 all-gather.10.cloned.1.call-update
  78.9 3.6 %all-to-all-start.1 = ((bf16[4,512,512]{2,1,0:T(8,128)(2,1)}), bf16[4,512,512]{2,1,0:T(8,128)(2,1)S(1)}, u32[]{:S(2)}, u32[]{:S(2)}) async-start(bf16[4,512,512]{2,1,0:T(8,128)(2,1)} %bitcast.13), calls=%async_computation.1 | async-start | bytes 4194304 | tf_op jit(solution)/shard_map/all_to_all | solution.py:43
  82.6 0.0 all-gather.12.cloned.1.call-start
  82.6 41.1 %all-gather.10.cloned.1.call-done = bf16[1024,512]{1,0:T(8,128)(2,1)} async-done(((bf16[256,512]{1,0:T(8,128)(2,1)}), bf16[1024,512]{1,0:T(8,128)(2,1)}) %all-gather.10.cloned.1.call-update) | async-done | bytes 1048592 | tf_op jit(solution)/shard_map/all_gather | solution.py:46
  123.8 0.0 all-gather.12.cloned.1.call-update
  123.8 4.0 %copy.10 = bf16[512,2048]{0,1:T(8,128)(2,1)} copy(bf16[512,2048]{1,0:T(8,128)(2,1)} %param.10) | data formatting | bytes 4194304 | tf_op args[4]
  127.7 20.0 %all-to-all-done.1 = bf16[4,512,512]{2,1,0:T(8,128)(2,1)S(1)} async-done(((bf16[4,512,512]{2,1,0:T(8,128)(2,1)}), bf16[4,512,512]{2,1,0:T(8,128)(2,1)S(1)}, u32[]{:S(2)}, u32[]{:S(2)}) %all-to-all-start.1) | async-done | bytes 2097184 | tf_op jit(solution)/shard_map/all_to_all | solution.py:43
  147.7 0.0 copy-start.2
  147.7 4.6 %all-to-all-start = ((bf16[512,4,512]{0,2,1:T(8,128)(2,1)}), bf16[512,4,512]{0,2,1:T(8,128)(2,1)}, u32[]{:S(2)}, u32[]{:S(2)}) async-start(bf16[512,4,512]{0,2,1:T(8,128)(2,1)} %bitcast.12), calls=%async_computation | async-start | bytes 4194304 | tf_op jit(solution)/shard_map/all_to_all | solution.py:42
  152.3 0.0 reduce-scatter.3.cloned.1.call-start
  152.3 0.0 copy-done.2
  152.4 5.4 %all-gather = bf16[4,1,512]{2,1,0:T(2,128)(2,1)S(1)} all-gather(bf16[1,1,512]{2,1,0:T(2,128)(2,1)S(1)} %reshape.15), channel_id=1, replica_groups=mesh['grp'=2,'fs'=4,'tp'=4] {'tp'}, dimensions={0}, use_global_device_ids=true | all-gather | bytes 5120 | tf_op jit(solution)/shard_map/all_gather | solution.py:48
  157.7 2.4 copy.12
  160.1 40.0 %all-to-all-done = bf16[512,4,512]{0,2,1:T(8,128)(2,1)} async-done(((bf16[512,4,512]{0,2,1:T(8,128)(2,1)}), bf16[512,4,512]{0,2,1:T(8,128)(2,1)}, u32[]{:S(2)}, u32[]{:S(2)}) %all-to-all-start) | async-done | bytes 2097184 | tf_op jit(solution)/shard_map/all_to_all | solution.py:42
  200.1 4.2 %copy.11 = bf16[4,512,512]{2,1,0:T(8,128)(2,1)} copy(bf16[4,512,512]{1,2,0:T(8,128)(2,1)} %bitcast.2) | data formatting | bytes 4194304 | tf_op jit(solution)/shard_map/all_to_all | solution.py:42
  204.3 0.0 copy-start
  204.3 0.0 all-gather.12.cloned.1.call-done
  204.3 3.2 %fusion = f32[1024]{0:T(1024)S(1)} fusion(bf16[1024,2048]{1,0:T(8,128)(2,1)} %all-gather.12.cloned.1.call-done), kind=kLoop, calls=%fused_computation.2 | loop fusion | flops 6290432 | bytes 4198400 | tf_op jit(solution)/shard_map/reduce_sum | solution.py:49
  207.5 0.0 copy-done
  207.6 9.4 %convolution_convert_fusion = bf16[1024,2048]{1,0:T(8,128)(2,1)} fusion(bf16[512,2048]{0,1:T(8,128)(2,1)S(1)} %bitcast.14, bf16[2048,512]{1,0:T(8,128)(2,1)} %bitcast.15, bf16[1024,2048]{1,0:T(8,128)(2,1)} %all-gather.12.cloned.1.call-done, f32[2048]{0:T(1024)S(1)} %bitcast.16, f32[1024]{0:T(1024)S(1)} %add_rsqrt_fusion), kind=kOutput, calls=%fused_computation.8 | convolution fusion | flops 4307025920 | bytes 12595200 | tf_op jit(solution)/shard_map/dot_general | solution.py:53
  217.0 0.0 copy-start.1
  217.0 0.0 reduce-scatter.3.cloned.1.call-update
  217.0 0.0 reduce-scatter.5.cloned.1.call-start
  217.0 43.6 %reduce-scatter.3.cloned.1.call-done = bf16[1024,512]{1,0:T(8,128)(2,1)} async-done(((bf16[1024,2048]{1,0:T(8,128)(2,1)}), bf16[1024,512]{1,0:T(8,128)(2,1)}) %reduce-scatter.3.cloned.1.call-update) | async-done | bytes 1048592 | tf_op jit(solution)/shard_map/reduce_scatter | solution.py:56
  260.6 0.0 reduce-scatter.5.cloned.1.call-update
  260.6 29.4 %reduce-scatter.5.cloned.1.call-done = bf16[256,512]{1,0:T(8,128)(2,1)} async-done(((bf16[1024,512]{1,0:T(8,128)(2,1)}), bf16[256,512]{1,0:T(8,128)(2,1)}) %reduce-scatter.5.cloned.1.call-update) | async-done | bytes 262160 | tf_op jit(solution)/shard_map/reduce_scatter | solution.py:57
  290.1 0.0 copy-done.1
  290.1 1.7 add_convert_fusion
  (3 shorter events, 0.0 us)
Async XLA Ops:
  6.5 21.8 %all-gather.6.cloned.1.call-start = ((), (), s32[]{:S(2)}) async-start(), calls=%async_computation.4 | async-start | bytes 1310720 | tf_op jit(solution)/shard_map/all_gather | solution.py:40
  7.3 68.3 %all-gather.8.cloned.1.call-start = ((), (), s32[]{:S(2)}) async-start(), calls=%async_computation.5 | async-start | bytes 2621440 | tf_op jit(solution)/shard_map/all_gather | solution.py:41
  8.0 115.8 %all-gather.10.cloned.1.call-start = ((), (), s32[]{:S(2)}) async-start(), calls=%async_computation.6 | async-start | bytes 1310720 | tf_op jit(solution)/shard_map/all_gather | solution.py:46
  78.9 68.8 %all-to-all-start.1 = ((bf16[4,512,512]{2,1,0:T(8,128)(2,1)}), bf16[4,512,512]{2,1,0:T(8,128)(2,1)S(1)}, u32[]{:S(2)}, u32[]{:S(2)}) async-start(bf16[4,512,512]{2,1,0:T(8,128)(2,1)} %bitcast.13), calls=%async_computation.1 | async-start | bytes 4194304 | tf_op jit(solution)/shard_map/all_to_all | solution.py:43
  82.6 121.7 %all-gather.12.cloned.1.call-start = ((), (), s32[]{:S(2)}) async-start(), calls=%async_computation.7 | async-start | bytes 5242880 | tf_op jit(solution)/shard_map/all_gather | solution.py:47
  147.7 4.7 %copy-start.2 = (bf16[512]{0:T(512)(128)(2,1)S(1)}, bf16[512]{0:T(512)(128)(2,1)}, u32[]{:S(2)}) copy-start(bf16[512]{0:T(512)(128)(2,1)} %param.9) | copy-start | bytes 3076
  147.7 52.4 %all-to-all-start = ((bf16[512,4,512]{0,2,1:T(8,128)(2,1)}), bf16[512,4,512]{0,2,1:T(8,128)(2,1)}, u32[]{:S(2)}, u32[]{:S(2)}) async-start(bf16[512,4,512]{0,2,1:T(8,128)(2,1)} %bitcast.12), calls=%async_computation | async-start | bytes 4194304 | tf_op jit(solution)/shard_map/all_to_all | solution.py:42
  152.3 108.3 %reduce-scatter.3.cloned.1.call-start = ((), (), s32[]{:S(2)}) async-start(), calls=%async_computation.8 | async-start | bytes 5242880 | tf_op jit(solution)/shard_map/reduce_scatter | solution.py:56
  204.3 3.2 %copy-start = (bf16[512,4,512]{0,2,1:T(8,128)(2,1)S(1)}, bf16[512,4,512]{0,2,1:T(8,128)(2,1)}, u32[]{:S(2)}) copy-start(bf16[512,4,512]{0,2,1:T(8,128)(2,1)} %copy.12) | copy-start | bytes 6291460
  217.0 73.1 %copy-start.1 = (bf16[256,512]{1,0:T(8,128)(2,1)S(1)}, bf16[256,512]{1,0:T(8,128)(2,1)}, u32[]{:S(2)}) copy-start(bf16[256,512]{1,0:T(8,128)(2,1)} %fusion.9) | copy-start | bytes 786436
  217.0 73.1 %reduce-scatter.5.cloned.1.call-start = ((), (), s32[]{:S(2)}) async-start(), calls=%async_computation.9 | async-start | bytes 1310720 | tf_op jit(solution)/shard_map/reduce_scatter | solution.py:57
Sparse Core Ops, SparseCore 0:
  8.9 19.4 all-gather.5
  29.9 45.6 all-gather.7
  79.1 44.6 all-gather.9
  125.2 47.2 all-gather.11
  217.1 43.4 reduce-scatter.2
  262.7 27.2 reduce-scatter.4
where the time goes:
time: 299 us
  waiting for transfers between devices  243 us (81%)
  between operations  13.5 us (5%)
  matrix products  12.7 us (4%)
  local copies, waits for them, and re-layouts  10.6 us (4%)
  starting transfers between devices  8.42 us (3%)
  blocking collectives  5.37 us (2%)
  other arithmetic  4.95 us (2%)
    all_gather x1, waiting for transfers between devices, spread_body(): out_full = lax.all_gather(out_weight, 'fs', axis=0, tiled=True)  47.3 us
    reduce_scatter x1, waiting for transfers between devices, spread_body(): columns = lax.psum_scatter(partials, 'tp', scatter_dimension=1, tiled=True)  43.6 us
    all_gather x1, waiting for transfers between devices, spread_body(): rows = lax.all_gather(resid, 'fs', axis=0, tiled=True)  41.1 us
    all_to_all x1, waiting for transfers between devices, spread_body(): lax.all_to_all(up_weight, 'fs', split_axis=1, concat_axis=0, tiled=True)  40 us
    reduce_scatter x1, waiting for transfers between devices, spread_body(): branch = lax.psum_scatter(columns, 'fs', scatter_dimension=0, tiled=True)  29.4 us
    all_gather x1, waiting for transfers between devices, spread_body(): mixed_whole = lax.all_gather(mixed, 'tp', axis=1, tiled=True)  20.3 us
    all_to_all x1, waiting for transfers between devices, spread_body(): lax.all_to_all(down_weight, 'fs', split_axis=0, concat_axis=1, tiled=True)  20 us
    dot_general x1, matrix products, spread_body(): jnp.dot(activated, down_mine, preferred_element_type=jnp.float32)  9.4 us
  transfers between devices with their start and end apart: 8, of which 7 were waited for; matrix products, arithmetic and copies ran while one was open for 4% of the time, Pallas kernels for 0%

commit v1 on v0

--- a/solution.py
+++ b/solution.py
@@ -37,7 +37,20 @@
 
 
 def spread_body(stream, mixed, out_weight, norm_gain, up_weight, down_weight):
-    mixed_whole = lax.all_gather(mixed, "tp", axis=1, tiled=True)
+
+    def cut_sector_on_mesh(inp, shard_axis, axis_no):
+        n_slots = lax.axis_size(shard_axis)
+        sides = tuple(((b, (b + 1) % n_slots) for b in range(n_slots)))
+        o_now = [None] * n_slots
+        o_now[n_slots - 1] = inp
+        for no in range(n_slots - 2, -1, -1):
+            o_now[no] = lax.ppermute(o_now[no + 1], shard_axis, sides)
+        step_out = jnp.concatenate(o_now, axis_no)
+        piece_next = lax.axis_index(shard_axis)
+        everything = jnp.roll(step_out, (piece_next + 1) * inp.shape[axis_no], axis_no)
+        return everything
+
+    mixed_whole = cut_sector_on_mesh(mixed, "tp", 1)
     out_full = lax.all_gather(out_weight, "fs", axis=0, tiled=True)
     up_mine = lax.all_to_all(up_weight, "fs", split_axis=1, concat_axis=0, tiled=True)
     down_mine = lax.all_to_all(down_weight, "fs", split_axis=0, concat_axis=1, tiled=True)

time: 299 us -> 280 us (0.936)
  waiting for transfers between devices: 243 us -> 224 us
    all_gather x1 -> x0, waiting for transfers between devices: 20.3 us -> none  [spread_body(): mixed_whole = lax.all_gather(mixed, 'tp', axis=1, tiled=True)]
    ppermute x0 -> x3, waiting for transfers between devices: none -> 17.8 us  [cut_sector_on_mesh(): o_now[no] = lax.ppermute(o_now[no + 1], shard_axis, sides)]
    all_gather x1, waiting for transfers between devices: 47.3 us -> 31.4 us  [spread_body(): out_full = lax.all_gather(out_weight, 'fs', axis=0, tiled=True)]
  transfers between devices with their start and end apart: 8 -> 10, of which waited for: 7 -> 9; matrix products, arithmetic and copies ran while one was open for 4% -> 4% of each run, Pallas kernels for 0% -> 0%
where the time goes in v1:
time: 280 us
  waiting for transfers between devices  224 us (80%)
  between operations  13.3 us (5%)
  matrix products  12.4 us (4%)
  local copies, waits for them, and re-layouts  10.8 us (4%)
  starting transfers between devices  8.96 us (3%)
  blocking collectives  5.36 us (2%)
  other arithmetic  4.95 us (2%)
    reduce_scatter x1, waiting for transfers between devices, spread_body(): columns = lax.psum_scatter(partials, 'tp', scatter_dimension=1, tiled=True)  43.5 us
    all_gather x1, waiting for transfers between devices, spread_body(): rows = lax.all_gather(resid, 'fs', axis=0, tiled=True)  41.1 us
    all_to_all x1, waiting for transfers between devices, spread_body(): lax.all_to_all(up_weight, 'fs', split_axis=1, concat_axis=0, tiled=True)  40 us
    all_gather x1, waiting for transfers between devices, spread_body(): out_full = lax.all_gather(out_weight, 'fs', axis=0, tiled=True)  31.4 us
    reduce_scatter x1, waiting for transfers between devices, spread_body(): branch = lax.psum_scatter(columns, 'fs', scatter_dimension=0, tiled=True)  29.4 us
    all_to_all x1, waiting for transfers between devices, spread_body(): lax.all_to_all(down_weight, 'fs', split_axis=0, concat_axis=1, tiled=True)  20 us
    ppermute x3, waiting for transfers between devices, cut_sector_on_mesh(): o_now[no] = lax.ppermute(o_now[no + 1], shard_axis, sides)  17.8 us
    dot_general x1, matrix products, spread_body(): jnp.dot(activated, down_mine, preferred_element_type=jnp.float32)  9.41 us
  transfers between devices with their start and end apart: 10, of which 9 were waited for; matrix products, arithmetic and copies ran while one was open for 4% of the time, Pallas kernels for 0%

profile of v1, /device:TPU:0, one launch (start us, length us, event | category | flops | bytes accessed | tf_op | source)
XLA Modules:
  0.0 279.7 jit_solution(2316502643768820807)
XLA Ops:
  6.5 0.0 copy-start.2
  6.5 0.0 all-gather.5.cloned.1.call-start
  6.5 0.7 all-gather.5.cloned.1.call-update
  7.3 0.0 all-gather.7.cloned.1.call-start
  7.3 0.5 collective-permute-start
  7.8 6.2 %collective-permute-done = bf16[256,512]{1,0:T(8,128)(2,1)S(1)} collective-permute-done((bf16[256,512]{1,0:T(8,128)(2,1)}, bf16[256,512]{1,0:T(8,128)(2,1)S(1)}, u32[]{:S(2)}, u32[]{:S(2)}) %collective-permute-start) | collective-permute-done | bytes 262176 | tf_op jit(solution)/shard_map/ppermute | solution.py:47
  14.1 0.0 collective-permute-start.1
  14.1 5.8 %collective-permute-done.1 = bf16[256,512]{1,0:T(8,128)(2,1)S(1)} collective-permute-done((bf16[256,512]{1,0:T(8,128)(2,1)S(1)}, bf16[256,512]{1,0:T(8,128)(2,1)S(1)}, u32[]{:S(2)}, u32[]{:S(2)}) %collective-permute-start.1) | collective-permute-done | bytes 262176 | tf_op jit(solution)/shard_map/ppermute | solution.py:47
  19.9 0.0 collective-permute-start.2
  19.9 0.0 copy-start.4
  19.9 5.8 %collective-permute-done.2 = bf16[256,512]{1,0:T(8,128)(2,1)S(1)} collective-permute-done((bf16[256,512]{1,0:T(8,128)(2,1)S(1)}, bf16[256,512]{1,0:T(8,128)(2,1)S(1)}, u32[]{:S(2)}, u32[]{:S(2)}) %collective-permute-start.2) | collective-permute-done | bytes 262176 | tf_op jit(solution)/shard_map/ppermute | solution.py:47
  25.8 0.0 copy-done.2
  25.9 31.4 %all-gather.5.cloned.1.call-done = bf16[2048,512]{1,0:T(8,128)(2,1)} async-done(((bf16[512,512]{1,0:T(8,128)(2,1)}), bf16[2048,512]{1,0:T(8,128)(2,1)}) %all-gather.5.cloned.1.call-update) | async-done | bytes 2097168 | tf_op jit(solution)/shard_map/all_gather | solution.py:54
  57.3 0.0 copy-done.4
  57.3 3.0 %fusion.9 = bf16[256,512]{1,0:T(8,128)(2,1)} fusion(bf16[2048,512]{1,0:T(8,128)(2,1)} %all-gather.5.cloned.1.call-done, bf16[256,4096]{1,0:T(8,128)(2,1)S(1)} %constant_dynamic-update-slice_fusion, s32[]{:T(128)S(6)} %select_n.14, bf16[256,512]{1,0:T(8,128)(2,1)S(1)} %copy-done.4), kind=kOutput, calls=%fused_computation.11 | convolution fusion | flops 537264128 | bytes 3670020 | tf_op jit(solution)/shard_map/dot_general | solution.py:57
  60.3 0.0 all-gather.7.cloned.1.call-update
  60.3 3.6 %all-to-all-start.1 = ((bf16[4,512,512]{2,1,0:T(8,128)(2,1)}), bf16[4,512,512]{2,1,0:T(8,128)(2,1)S(1)}, u32[]{:S(2)}, u32[]{:S(2)}) async-start(bf16[4,512,512]{2,1,0:T(8,128)(2,1)} %bitcast.12), calls=%async_computation.1 | async-start | bytes 4194304 | tf_op jit(solution)/shard_map/all_to_all | solution.py:56
  64.0 0.0 all-gather.9.cloned.1.call-start
  64.0 41.1 %all-gather.7.cloned.1.call-done = bf16[1024,512]{1,0:T(8,128)(2,1)} async-done(((bf16[256,512]{1,0:T(8,128)(2,1)}), bf16[1024,512]{1,0:T(8,128)(2,1)}) %all-gather.7.cloned.1.call-update) | async-done | bytes 1048592 | tf_op jit(solution)/shard_map/all_gather | solution.py:59
  105.2 0.0 all-gather.9.cloned.1.call-update
  105.2 3.9 %copy.10 = bf16[512,2048]{0,1:T(8,128)(2,1)} copy(bf16[512,2048]{1,0:T(8,128)(2,1)} %param.10) | data formatting | bytes 4194304 | tf_op args[4]
  109.1 20.0 %all-to-all-done.1 = bf16[4,512,512]{2,1,0:T(8,128)(2,1)S(1)} async-done(((bf16[4,512,512]{2,1,0:T(8,128)(2,1)}), bf16[4,512,512]{2,1,0:T(8,128)(2,1)S(1)}, u32[]{:S(2)}, u32[]{:S(2)}) %all-to-all-start.1) | async-done | bytes 2097184 | tf_op jit(solution)/shard_map/all_to_all | solution.py:56
  129.1 0.0 copy-start.3
  129.1 4.6 %all-to-all-start = ((bf16[512,4,512]{0,2,1:T(8,128)(2,1)}), bf16[512,4,512]{0,2,1:T(8,128)(2,1)}, u32[]{:S(2)}, u32[]{:S(2)}) async-start(bf16[512,4,512]{0,2,1:T(8,128)(2,1)} %bitcast.11), calls=%async_computation | async-start | bytes 4194304 | tf_op jit(solution)/shard_map/all_to_all | solution.py:55
  133.7 0.0 reduce-scatter.3.cloned.1.call-start
  133.7 0.0 copy-done.3
  133.8 5.4 %all-gather = bf16[4,1,512]{2,1,0:T(2,128)(2,1)S(1)} all-gather(bf16[1,1,512]{2,1,0:T(2,128)(2,1)S(1)} %reshape.15), channel_id=1, replica_groups=mesh['grp'=2,'fs'=4,'tp'=4] {'tp'}, dimensions={0}, use_global_device_ids=true | all-gather | bytes 5120 | tf_op jit(solution)/shard_map/all_gather | solution.py:61
  139.1 2.4 copy.12
  141.5 40.0 %all-to-all-done = bf16[512,4,512]{0,2,1:T(8,128)(2,1)} async-done(((bf16[512,4,512]{0,2,1:T(8,128)(2,1)}), bf16[512,4,512]{0,2,1:T(8,128)(2,1)}, u32[]{:S(2)}, u32[]{:S(2)}) %all-to-all-start) | async-done | bytes 2097184 | tf_op jit(solution)/shard_map/all_to_all | solution.py:55
  181.5 4.2 %copy.11 = bf16[4,512,512]{2,1,0:T(8,128)(2,1)} copy(bf16[4,512,512]{1,2,0:T(8,128)(2,1)} %bitcast.2) | data formatting | bytes 4194304 | tf_op jit(solution)/shard_map/all_to_all | solution.py:55
  185.7 0.0 copy-start
  185.7 0.0 all-gather.9.cloned.1.call-done
  185.7 3.2 %fusion = f32[1024]{0:T(1024)S(1)} fusion(bf16[1024,2048]{1,0:T(8,128)(2,1)} %all-gather.9.cloned.1.call-done), kind=kLoop, calls=%fused_computation.2 | loop fusion | flops 6290432 | bytes 4198400 | tf_op jit(solution)/shard_map/reduce_sum | solution.py:62
  188.9 0.0 copy-done
  189.0 9.4 %convolution_convert_fusion = bf16[1024,2048]{1,0:T(8,128)(2,1)} fusion(bf16[512,2048]{0,1:T(8,128)(2,1)S(1)} %bitcast.13, bf16[2048,512]{1,0:T(8,128)(2,1)} %bitcast.14, bf16[1024,2048]{1,0:T(8,128)(2,1)} %all-gather.9.cloned.1.call-done, f32[2048]{0:T(1024)S(1)} %bitcast.15, f32[1024]{0:T(1024)S(1)} %add_rsqrt_fusion), kind=kOutput, calls=%fused_computation.8 | convolution fusion | flops 4307025920 | bytes 12595200 | tf_op jit(solution)/shard_map/dot_general | solution.py:66
  198.4 0.0 copy-start.1
  198.4 0.0 reduce-scatter.3.cloned.1.call-update
  198.4 0.0 reduce-scatter.5.cloned.1.call-start
  198.4 43.5 %reduce-scatter.3.cloned.1.call-done = bf16[1024,512]{1,0:T(8,128)(2,1)} async-done(((bf16[1024,2048]{1,0:T(8,128)(2,1)}), bf16[1024,512]{1,0:T(8,128)(2,1)}) %reduce-scatter.3.cloned.1.call-update) | async-done | bytes 1048592 | tf_op jit(solution)/shard_map/reduce_scatter | solution.py:69
  242.0 0.0 reduce-scatter.5.cloned.1.call-update
  242.0 29.4 %reduce-scatter.5.cloned.1.call-done = bf16[256,512]{1,0:T(8,128)(2,1)} async-done(((bf16[1024,512]{1,0:T(8,128)(2,1)}), bf16[256,512]{1,0:T(8,128)(2,1)}) %reduce-scatter.5.cloned.1.call-update) | async-done | bytes 262160 | tf_op jit(solution)/shard_map/reduce_scatter | solution.py:70
  271.4 0.0 copy-done.1
  271.4 1.7 add_convert_fusion
  (11 shorter events, 0.2 us)
Async XLA Ops:
  6.5 19.2 %copy-start.2 = (bf16[256,512]{1,0:T(8,128)(2,1)S(1)}, bf16[256,512]{1,0:T(8,128)(2,1)}, u32[]{:S(2)}) copy-start(bf16[256,512]{1,0:T(8,128)(2,1)} %param.7) | copy-start | bytes 786436
  6.5 50.8 %all-gather.5.cloned.1.call-start = ((), (), s32[]{:S(2)}) async-start(), calls=%async_computation.4 | async-start | bytes 2621440 | tf_op jit(solution)/shard_map/all_gather | solution.py:54
  7.3 97.9 %all-gather.7.cloned.1.call-start = ((), (), s32[]{:S(2)}) async-start(), calls=%async_computation.5 | async-start | bytes 1310720 | tf_op jit(solution)/shard_map/all_gather | solution.py:59
  7.3 6.8 %collective-permute-start = (bf16[256,512]{1,0:T(8,128)(2,1)}, bf16[256,512]{1,0:T(8,128)(2,1)S(1)}, u32[]{:S(2)}, u32[]{:S(2)}) collective-permute-start(bf16[256,512]{1,0:T(8,128)(2,1)} %param.7), channel_id=1, source_target_pairs={{0,1},{1,2},{2,3},{3,0},{4,5},{5,6},{6,7},{7,4},{8,9},{9,10},{10,1... | collective-permute-start | bytes 786440 | tf_op jit(solution)/shard_map/ppermute | solution.py:47
  14.1 5.8 %collective-permute-start.1 = (bf16[256,512]{1,0:T(8,128)(2,1)S(1)}, bf16[256,512]{1,0:T(8,128)(2,1)S(1)}, u32[]{:S(2)}, u32[]{:S(2)}) collective-permute-start(bf16[256,512]{1,0:T(8,128)(2,1)S(1)} %collective-permute-done), channel_id=1, source_target_pairs={{0,1},{1,2},{2,3},{3,0},{4,5},{5,6},{6,7},{7,4},{8,9},{9,10},{10,1... | collective-permute-start | bytes 786440 | tf_op jit(solution)/shard_map/ppermute | solution.py:47
  19.9 5.8 %collective-permute-start.2 = (bf16[256,512]{1,0:T(8,128)(2,1)S(1)}, bf16[256,512]{1,0:T(8,128)(2,1)S(1)}, u32[]{:S(2)}, u32[]{:S(2)}) collective-permute-start(bf16[256,512]{1,0:T(8,128)(2,1)S(1)} %collective-permute-done.1), channel_id=1, source_target_pairs={{0,1},{1,2},{2,3},{3,0},{4,5},{5,6},{6,7},{7,4},{8,9},{9,10},{10,1... | collective-permute-start | bytes 786440 | tf_op jit(solution)/shard_map/ppermute | solution.py:47
  19.9 37.5 %copy-start.4 = (bf16[256,512]{1,0:T(8,128)(2,1)S(1)}, bf16[256,512]{1,0:T(8,128)(2,1)}, u32[]{:S(2)}) copy-start(bf16[256,512]{1,0:T(8,128)(2,1)} %param.6) | copy-start | bytes 786436
  60.3 68.8 %all-to-all-start.1 = ((bf16[4,512,512]{2,1,0:T(8,128)(2,1)}), bf16[4,512,512]{2,1,0:T(8,128)(2,1)S(1)}, u32[]{:S(2)}, u32[]{:S(2)}) async-start(bf16[4,512,512]{2,1,0:T(8,128)(2,1)} %bitcast.12), calls=%async_computation.1 | async-start | bytes 4194304 | tf_op jit(solution)/shard_map/all_to_all | solution.py:56
  64.0 121.7 %all-gather.9.cloned.1.call-start = ((), (), s32[]{:S(2)}) async-start(), calls=%async_computation.6 | async-start | bytes 5242880 | tf_op jit(solution)/shard_map/all_gather | solution.py:60
  129.1 4.6 %copy-start.3 = (bf16[512]{0:T(512)(128)(2,1)S(1)}, bf16[512]{0:T(512)(128)(2,1)}, u32[]{:S(2)}) copy-start(bf16[512]{0:T(512)(128)(2,1)} %param.9) | copy-start | bytes 3076
  129.1 52.4 %all-to-all-start = ((bf16[512,4,512]{0,2,1:T(8,128)(2,1)}), bf16[512,4,512]{0,2,1:T(8,128)(2,1)}, u32[]{:S(2)}, u32[]{:S(2)}) async-start(bf16[512,4,512]{0,2,1:T(8,128)(2,1)} %bitcast.11), calls=%async_computation | async-start | bytes 4194304 | tf_op jit(solution)/shard_map/all_to_all | solution.py:55
  133.7 108.3 %reduce-scatter.3.cloned.1.call-start = ((), (), s32[]{:S(2)}) async-start(), calls=%async_computation.7 | async-start | bytes 5242880 | tf_op jit(solution)/shard_map/reduce_scatter | solution.py:69
  185.7 3.2 %copy-start = (bf16[512,4,512]{0,2,1:T(8,128)(2,1)S(1)}, bf16[512,4,512]{0,2,1:T(8,128)(2,1)}, u32[]{:S(2)}) copy-start(bf16[512,4,512]{0,2,1:T(8,128)(2,1)} %copy.12) | copy-start | bytes 6291460
  198.4 73.1 %copy-start.1 = (bf16[256,512]{1,0:T(8,128)(2,1)S(1)}, bf16[256,512]{1,0:T(8,128)(2,1)}, u32[]{:S(2)}) copy-start(bf16[256,512]{1,0:T(8,128)(2,1)} %fusion.9) | copy-start | bytes 786436
  198.4 73.0 %reduce-scatter.5.cloned.1.call-start = ((), (), s32[]{:S(2)}) async-start(), calls=%async_computation.8 | async-start | bytes 1310720 | tf_op jit(solution)/shard_map/reduce_scatter | solution.py:70
Sparse Core Ops, SparseCore 0:
  8.9 48.3 all-gather.4
  60.5 44.6 all-gather.6
  106.7 47.2 all-gather.8
  198.5 43.4 reduce-scatter.2
  244.1 27.2 reduce-scatter.4
